TPU v7x, 256 devices: a whole 4x4x8 slice. The times are simulated.
256 devices in a mesh: ep: 64 (over z, y, core), tp: 4 (over x).
Axes of the slice: x: 4, y: 4, z: 8, core: 2. Of those that a mesh axis runs over, the one named last changes fastest.
Arguments:
- c_gate: bfloat16 [16384, 1024], P('ep', 'tp'), may hold values from -6 to 6
- b_gate: bfloat16 [16384, 1024], P('ep', 'tp'), may hold values from -6 to 6
- values: bfloat16 [16384, 1024], P('ep', 'tp'), may hold values from -6 to 6
- conv_taps: float32 [3, 1024], P(None, 'tp'), may hold values from -3.5 to 3.5
- w_mix_out: bfloat16 [1024, 2048], P('tp'), may hold values from -0.1875 to 0.1875
- moe_in: bfloat16 [32768, 2048], P(('ep', 'tp')), may hold values from -6 to 6
- norm_gain: float32 [2048], replicated, may hold values from 0.1 to 1.9
- route_ids: int32 [32768, 2], P(('ep', 'tp')), may hold values from 0 to 63, all different within a row; in each aligned block of 128 rows (0 to 127, 128 to 255, ...) at most 5 rows name the same one
- route_weights: float32 [32768, 2], P(('ep', 'tp')), may hold values from 0.1 to 1
- w_gate: bfloat16 [64, 2048, 3584], P('ep', None, 'tp'), may hold values from -0.125 to 0.125
- w_up: bfloat16 [64, 2048, 3584], P('ep', None, 'tp'), may hold values from -0.125 to 0.125
- w_down: bfloat16 [64, 3584, 2048], P('ep', 'tp'), may hold values from -0.09375 to 0.09375
Outputs:
- mixer_out: bfloat16 [16384, 2048], P(('ep', 'tp'))
- moe_out: bfloat16 [32768, 2048], P(('ep', 'tp'))
Inputs may be any that keep to these rules, and one draw needn't show every extreme that they name: `route_ids`: each row names 2 different experts; in each aligned block of 128 rows (the rows of one device) no expert is named by more than 5 rows, and in every draw some expert is named by exactly 5 rows in some block.
All inputs are finite; a program needn't handle non-finite values.
Results may differ from a plain program's by a relative error of at most 0.012.
Values may be sent and summed in bfloat16 or wider, within the bound.
No kernel may reach another device: no remote copies, remote signals or barrier semaphores. Data moves between devices by JAX's collectives and lax.ppermute only.
A program may use at most 128 MiB of HBM per device.

v0:
```python
import jax
import jax.numpy as jnp
from jax import lax
from jax.sharding import PartitionSpec as P

EPS = 1e-06


def passed_along(block, axis, distance):
    devices = range(lax.axis_size(axis))
    route = [(i - distance, i) for i in devices if i - distance in devices]
    return lax.ppermute(block, axis, route)


def split_up(shard, dim, length):
    before, after = (shard.shape[:dim], shard.shape[dim + 1 :])
    return jnp.moveaxis(shard.reshape(*before, length, -1, *after), dim, 0)


def sent_and_summed(shard, axis, dim):
    blocks = split_up(shard, dim, lax.axis_size(axis))
    arrived = lax.all_to_all(blocks, axis, split_axis=0, concat_axis=0, tiled=True)
    return arrived.astype(jnp.float32).sum(axis=0)


def rank_copies(route_block, experts):
    flat_ids = route_block.reshape(-1)
    onehot = (flat_ids[:, None] == jnp.arange(experts, dtype=jnp.int32)[None, :]).astype(jnp.int32)
    before = jnp.cumsum(onehot, axis=0) - onehot
    return (flat_ids, jnp.sum(before * onehot, axis=1))


def pack_rows(rows, slot_of, top, slot_count):
    copies = slot_of.shape[0]
    table = (
        jnp.full((slot_count,), copies, jnp.int32)
        .at[slot_of]
        .set(jnp.arange(copies, dtype=jnp.int32))
    )
    padded = jnp.concatenate([rows, jnp.zeros((1, rows.shape[1]), rows.dtype)], 0)
    return padded[table // top]


def on_device(
    c_gate,
    b_gate,
    values,
    conv_taps,
    w_mix_out,
    moe_in,
    norm_gain,
    route_ids,
    route_weights,
    w_gate,
    w_up,
    w_down,
):
    tokens = c_gate.shape[0]
    reach = conv_taps.shape[0] - 1
    product = c_gate.astype(jnp.float32) * values.astype(jnp.float32)
    previous = passed_along(product[tokens - reach :], "ep", 1)
    extended = jnp.concatenate([previous, product], 0)
    convolved = jnp.zeros_like(product)
    for offset in range(reach + 1):
        convolved = convolved + conv_taps[offset][None, :] * extended[offset : offset + tokens]
    mixed = (b_gate.astype(jnp.float32) * convolved).astype(jnp.bfloat16)
    piece = mixed
    mixer_out = sent_and_summed(
        jnp.dot(piece, w_mix_out, preferred_element_type=jnp.float32).astype(jnp.bfloat16), "tp", 0
    ).astype(jnp.bfloat16)
    rows_b = moe_in.shape[0]
    width = moe_in.shape[1]
    top = route_ids.shape[1]
    n_ep = lax.axis_size("ep")
    experts = w_gate.shape[0] * n_ep
    capacity = 5 * rows_b * top // (4 * experts)
    stream = moe_in.astype(jnp.float32)
    scale = lax.rsqrt(jnp.mean(stream * stream, axis=1, keepdims=True) + EPS)
    normed = (stream * scale * norm_gain[None, :]).astype(jnp.bfloat16)
    own_ids, own_ranks = rank_copies(route_ids, experts)
    own_slot = own_ids * capacity + own_ranks
    outgoing = pack_rows(normed, own_slot, top, experts * capacity).reshape(
        experts, capacity, width
    )
    arrived = lax.all_to_all(outgoing, "ep", split_axis=0, concat_axis=1, tiled=True).reshape(
        -1, width
    )
    piece = lax.all_gather(arrived, "tp", axis=0, tiled=True)
    gate_val = jnp.dot(piece, w_gate[0], preferred_element_type=jnp.float32)
    up_val = jnp.dot(piece, w_up[0], preferred_element_type=jnp.float32)
    hidden = (jax.nn.silu(gate_val) * up_val).astype(jnp.bfloat16)
    piece = hidden
    expert_out = sent_and_summed(
        jnp.dot(piece, w_down[0], preferred_element_type=jnp.float32).astype(jnp.bfloat16), "tp", 0
    ).astype(jnp.bfloat16)
    returned = lax.all_to_all(
        expert_out.reshape(n_ep, capacity, width), "ep", split_axis=0, concat_axis=0, tiled=True
    )
    picked = returned.reshape(-1, width)[own_slot].astype(jnp.float32).reshape(rows_b, top, width)
    moe_out = jnp.sum(picked * route_weights[:, :, None], axis=1).astype(jnp.bfloat16)
    return (mixer_out, moe_out)


def solution(mesh):
    return jax.shard_map(
        on_device,
        mesh=mesh,
        in_specs=(
            P("ep", "tp"),
            P("ep", "tp"),
            P("ep", "tp"),
            P(None, "tp"),
            P("tp", None),
            P(("ep", "tp"), None),
            P(),
            P(("ep", "tp"), None),
            P(("ep", "tp"), None),
            P("ep", None, "tp"),
            P("ep", None, "tp"),
            P("ep", "tp", None),
        ),
        out_specs=(P(("ep", "tp"), None), P(("ep", "tp"), None)),
        check_vma=False,
    )
```

profile of v0, /device:TPU:8, one launch (start us, length us, event | category | flops | bytes accessed | tf_op | source)
XLA Modules:
  0.0 333.2 jit_solution(17508996634302096302)
XLA Ops:
  10.3 1.4 scatter_custom_fusion
  13.0 1.2 fusion.6
  14.3 3.0 gather_fusion
  17.3 2.4 reshape.88
  19.7 63.2 %all_to_all.24 = bf16[64,5,2048]{2,1,0:T(8,128)(2,1)} all-to-all(bf16[64,5,2048]{2,1,0:T(8,128)(2,1)S(1)} %reshape.88), channel_id=1, replica_groups=mesh['ep'=64,'tp'=4] {'ep'}, dimensions={0} | all-to-all | bytes 2621440 | tf_op jit(solution)/shard_map/all_to_all | solution.py:85
  82.9 3.7 %reshape.89 = bf16[320,2048]{1,0:T(8,128)(2,1)} reshape(bf16[64,5,2048]{2,1,0:T(8,128)(2,1)} %all_to_all.24) | data formatting | bytes 2621440 | tf_op jit(solution)/shard_map/reshape | solution.py:85
  86.6 55.8 %all-gather.2.cloned.1.call-done = bf16[1280,2048]{1,0:T(8,128)(2,1)} async-done(((bf16[320,2048]{1,0:T(8,128)(2,1)}), bf16[1280,2048]{1,0:T(8,128)(2,1)}) %all-gather.2.cloned.1.call-update) | async-done | bytes 5242896 | tf_op jit(solution)/shard_map/all_gather | solution.py:88
  142.4 10.0 %fusion.2 = f32[1280,896]{1,0:T(8,128)} fusion(bf16[1280,2048]{1,0:T(8,128)(2,1)} %all-gather.2.cloned.1.call-done, bf16[1,2048,896]{2,1,0:T(8,128)(2,1)} %param.21), kind=kOutput, calls=%fused_computation.7 | convolution fusion | flops 4697620480 | bytes 13500416 | tf_op jit(solution)/shard_map/dot_general | solution.py:89
  152.4 17.5 %convolution_convert_fusion = bf16[1280,2048]{1,0:T(8,128)(2,1)} fusion(bf16[1,896,2048]{2,1,0:T(8,128)(2,1)} %param.23, f32[1280,896]{1,0:T(8,128)} %fusion.2, bf16[1280,2048]{1,0:T(8,128)(2,1)} %all-gather.2.cloned.1.call-done, bf16[1,2048,896]{2,1,0:T(8,128)(2,1)} %param.22), kind=kOutput, calls=%fused_computation.3 | convolution fusion | flops 9404743680 | bytes 22413312 | tf_op jit(solution)/shard_map/dot_general | solution.py:94
  169.9 5.2 %all-to-all-start.2 = ((bf16[4,320,2048]{2,1,0:T(8,128)(2,1)}), bf16[4,320,2048]{2,1,0:T(8,128)(2,1)}, u32[]{:S(2)}, u32[]{:S(2)}) async-start(bf16[4,320,2048]{2,1,0:T(8,128)(2,1)} %bitcast.47), calls=%async_computation.2 | async-start | bytes 10485760 | tf_op jit(solution)/shard_map/all_to_all | solution.py:22
  175.2 1.9 collective-permute-start
  177.2 3.0 collective-permute-done
  180.1 1.5 convolution_convert_fusion.1
  181.6 53.8 %all-to-all-done.2 = bf16[4,320,2048]{2,1,0:T(8,128)(2,1)} async-done(((bf16[4,320,2048]{2,1,0:T(8,128)(2,1)}), bf16[4,320,2048]{2,1,0:T(8,128)(2,1)}, u32[]{:S(2)}, u32[]{:S(2)}) %all-to-all-start.2) | async-done | bytes 5242912 | tf_op jit(solution)/shard_map/all_to_all | solution.py:22
  235.4 3.7 %all-to-all-start = ((bf16[4,64,2048]{2,1,0:T(8,128)(2,1)}), bf16[4,64,2048]{2,1,0:T(8,128)(2,1)S(1)}, u32[]{:S(2)}, u32[]{:S(2)}) async-start(bf16[4,64,2048]{2,1,0:T(8,128)(2,1)} %bitcast.3), calls=%async_computation | async-start | bytes 2097152 | tf_op jit(solution)/shard_map/all_to_all | solution.py:22
  239.1 3.6 %reduce_sum.57 = bf16[320,2048]{1,0:T(8,128)(2,1)S(1)} reduce(bf16[4,320,2048]{2,1,0:T(8,128)(2,1)} %all-to-all-done.2, bf16[]{:T(256)} %constant.18.clone.1), dimensions={0}, to_apply=%region_6.7 | reduce | flops 1966080 | bytes 6553602 | tf_op jit(solution)/shard_map/reduce_sum | solution.py:23
  242.7 1.6 reshape.91
  244.3 8.9 %all-to-all-done = bf16[4,64,2048]{2,1,0:T(8,128)(2,1)S(1)} async-done(((bf16[4,64,2048]{2,1,0:T(8,128)(2,1)}), bf16[4,64,2048]{2,1,0:T(8,128)(2,1)S(1)}, u32[]{:S(2)}, u32[]{:S(2)}) %all-to-all-start) | async-done | bytes 1048608 | tf_op jit(solution)/shard_map/all_to_all | solution.py:22
  253.2 10.7 %all-to-all-start.3 = ((bf16[64,5,2048]{2,1,0:T(8,128)(2,1)}), bf16[64,5,2048]{2,1,0:T(8,128)(2,1)}, u32[]{:S(2)}, u32[]{:S(2)}) async-start(bf16[64,5,2048]{2,1,0:T(8,128)(2,1)} %reshape.91), calls=%async_computation.3 | async-start | bytes 4194304 | tf_op jit(solution)/shard_map/all_to_all | solution.py:96
  265.0 50.1 %all-to-all-done.3 = bf16[64,5,2048]{2,1,0:T(8,128)(2,1)} async-done(((bf16[64,5,2048]{2,1,0:T(8,128)(2,1)}), bf16[64,5,2048]{2,1,0:T(8,128)(2,1)}, u32[]{:S(2)}, u32[]{:S(2)}) %all-to-all-start.3) | async-done | bytes 1310752 | tf_op jit(solution)/shard_map/all_to_all | solution.py:96
  315.1 2.6 reshape.92
  317.7 2.3 gather_fusion.1
  320.0 2.4 reshape.93
  322.4 3.9 %multiply_reduce_fusion = bf16[128,2048]{1,0:T(8,128)(2,1)} fusion(f32[128,2,2048]{2,1,0:T(2,128)S(1)} %reshape.93, f32[128,2]{1,0:T(8,128)S(1)} %copy.19), kind=kLoop, calls=%fused_computation.10 | loop fusion | flops 786432 | bytes 2622464 | tf_op jit(solution)/shard_map/reduce_sum | solution.py:100
  (39 shorter events, 5.5 us)
Async XLA Ops:
  7.2 173.0 %copy-start = (bf16[256,2048]{1,0:T(8,128)(2,1)S(1)}, bf16[256,2048]{1,0:T(8,128)(2,1)}, u32[]{:S(2)}) copy-start(bf16[256,2048]{1,0:T(8,128)(2,1)} %param.16) | copy-start | bytes 3145732
  7.2 135.2 %all-gather.2.cloned.1.call-start = ((), (), s32[]{:S(2)}) async-start(), calls=%async_computation.4 | async-start | bytes 6553600 | tf_op jit(solution)/shard_map/all_gather | solution.py:88
  169.9 5.3 %copy-start.2 = (bf16[256,256]{1,0:T(8,128)(2,1)S(1)}, bf16[256,256]{1,0:T(8,128)(2,1)}, u32[]{:S(2)}) copy-start(bf16[256,256]{1,0:T(8,128)(2,1)} %param.14) | copy-start | bytes 393220
  169.9 5.3 %copy-start.3 = (bf16[256,256]{1,0:T(8,128)(2,1)S(1)}, bf16[256,256]{1,0:T(8,128)(2,1)}, u32[]{:S(2)}) copy-start(bf16[256,256]{1,0:T(8,128)(2,1)} %param.12) | copy-start | bytes 393220
  169.9 7.2 %copy-start.4 = (f32[3,256]{1,0:T(4,128)S(1)}, f32[3,256]{1,0:T(4,128)}, u32[]{:S(2)}) copy-start(f32[3,256]{1,0:T(4,128)} %param.15) | copy-start | bytes 9220
  169.9 10.2 %copy-start.1 = (bf16[256,256]{1,0:T(8,128)(2,1)S(1)}, bf16[256,256]{1,0:T(8,128)(2,1)}, u32[]{:S(2)}) copy-start(bf16[256,256]{1,0:T(8,128)(2,1)} %param.13) | copy-start | bytes 393220
  169.9 65.4 %all-to-all-start.2 = ((bf16[4,320,2048]{2,1,0:T(8,128)(2,1)}), bf16[4,320,2048]{2,1,0:T(8,128)(2,1)}, u32[]{:S(2)}, u32[]{:S(2)}) async-start(bf16[4,320,2048]{2,1,0:T(8,128)(2,1)} %bitcast.47), calls=%async_computation.2 | async-start | bytes 10485760 | tf_op jit(solution)/shard_map/all_to_all | solution.py:22
  175.2 4.9 %collective-permute-start = (f32[2,256]{1,0:T(2,128)S(1)}, f32[2,256]{1,0:T(2,128)S(1)}, u32[]{:S(2)}, u32[]{:S(2)}) collective-permute-start(f32[2,256]{1,0:T(2,128)S(1)} %slice.36), channel_id=1, source_target_pairs={{0,4},{4,8},{8,12},{12,16},{16,20},{20,24},{24,28},{28,32},{32,36}... | collective-permute-start | bytes 6152 | tf_op jit(solution)/shard_map/ppermute | solution.py:12
  235.4 17.8 %all-to-all-start = ((bf16[4,64,2048]{2,1,0:T(8,128)(2,1)}), bf16[4,64,2048]{2,1,0:T(8,128)(2,1)S(1)}, u32[]{:S(2)}, u32[]{:S(2)}) async-start(bf16[4,64,2048]{2,1,0:T(8,128)(2,1)} %bitcast.3), calls=%async_computation | async-start | bytes 2097152 | tf_op jit(solution)/shard_map/all_to_all | solution.py:22
  242.7 21.3 %copy-start.5 = (f32[128,2]{0,1:T(2,128)S(1)}, f32[128,2]{0,1:T(2,128)}, u32[]{:S(2)}) copy-start(f32[128,2]{0,1:T(2,128)} %param.20) | copy-start | bytes 3076
  253.2 61.9 %all-to-all-start.3 = ((bf16[64,5,2048]{2,1,0:T(8,128)(2,1)}), bf16[64,5,2048]{2,1,0:T(8,128)(2,1)}, u32[]{:S(2)}, u32[]{:S(2)}) async-start(bf16[64,5,2048]{2,1,0:T(8,128)(2,1)} %reshape.91), calls=%async_computation.3 | async-start | bytes 4194304 | tf_op jit(solution)/shard_map/all_to_all | solution.py:96
Sparse Core Ops, SparseCore 0:
  86.7 55.6 all-gather.1
where the time goes:
time: 334 us; the launch traced here: 333 us
  waiting for transfers between devices  172 us (51%)
  blocking collectives  63.2 us (19%)
  matrix products  29 us (9%)
  starting transfers between devices  21.6 us (6%)
  local copies, waits for them, and re-layouts  21.1 us (6%)
  between operations  14.2 us (4%)
  other arithmetic  12.4 us (4%)
    all_to_all x1, blocking collectives, on_device(): lax.all_to_all(outgoing, 'ep', split_axis=0, concat_axis=1, tiled=True)  63.2 us
    all_to_all x2, waiting for transfers between devices, sent_and_summed(): lax.all_to_all(blocks, axis, split_axis=0, concat_axis=0, tiled=True)  62.6 us
    all_gather x1, waiting for transfers between devices, on_device(): piece = lax.all_gather(arrived, 'tp', axis=0, tiled=True)  55.8 us
    all_to_all x1, waiting for transfers between devices, on_device(): lax.all_to_all(expert_out.reshape(n_ep, capacity, width), 'ep', split_axi...  50.1 us
    dot_general x1, matrix products, on_device(): jnp.dot(piece, w_down[0], preferred_element_type=jnp.float32)  17.5 us
    all_to_all x1, starting transfers between devices, on_device(): lax.all_to_all(expert_out.reshape(n_ep, capacity, width), 'ep', split_axi...  10.7 us
    dot_general x1, matrix products, on_device(): gate_val = jnp.dot(piece, w_gate[0], preferred_element_type=jnp.float32)  9.98 us
    all_to_all x2, starting transfers between devices, sent_and_summed(): lax.all_to_all(blocks, axis, split_axis=0, concat_axis=0, tiled=True)  8.91 us
  transfers between devices with their start and end apart: 5, of which 5 were waited for; matrix products, arithmetic and copies ran while one was open for 2% of the time, Pallas kernels for 0%

commit v1 on v0

--- a/solution.py
+++ b/solution.py
@@ -85,7 +85,35 @@
     arrived = lax.all_to_all(outgoing, "ep", split_axis=0, concat_axis=1, tiled=True).reshape(
         -1, width
     )
-    piece = lax.all_gather(arrived, "tp", axis=0, tiled=True)
+
+    def threads_balance(field_in, mesh_dim):
+        piece_out, odd, low = (
+            jax.lax.axis_size(mesh_dim),
+            jax.lax.axis_index(mesh_dim),
+            field_in.shape[0],
+        )
+        d_next = tuple(
+            (dev_j * piece_out if q == 0 else dev_j for q, dev_j in enumerate(field_in.shape))
+        )
+        arr_next = jnp.zeros(d_next, field_in.dtype)
+        near = lax.dynamic_update_slice_in_dim(arr_next, field_in, odd * low, axis=0)
+        step_out = v_now = field_in
+        for h in [*range(1, piece_out // 2 + 1)]:
+            step_out = jax.lax.ppermute(
+                step_out, mesh_dim, perm=tuple(((q, (q + 1) % piece_out) for q in range(piece_out)))
+            )
+            near = lax.dynamic_update_slice_in_dim(
+                near, step_out, (odd - h) % piece_out * low, axis=0
+            )
+            if 2 * h < piece_out:
+                out_arr = tuple(((q, (q - 1) % piece_out) for q in range(piece_out)))
+                v_now = jax.lax.ppermute(v_now, mesh_dim, perm=out_arr)
+                near = lax.dynamic_update_slice_in_dim(
+                    near, v_now, (odd + h) % piece_out * low, axis=0
+                )
+        return near
+
+    piece = threads_balance(arrived, "tp")
     gate_val = jnp.dot(piece, w_gate[0], preferred_element_type=jnp.float32)
     up_val = jnp.dot(piece, w_up[0], preferred_element_type=jnp.float32)
     hidden = (jax.nn.silu(gate_val) * up_val).astype(jnp.bfloat16)

time: 334 us -> 322 us (0.964)
  between operations: 14.2 us -> 0.93 us
  waiting for transfers between devices: 172 us -> 162 us
  starting transfers between devices: 21.6 us -> 28.9 us
  local copies, waits for them, and re-layouts: 21.1 us -> 27.7 us
    all_gather x1 -> x0, waiting for transfers between devices: 55.8 us -> none  [on_device(): piece = lax.all_gather(arrived, 'tp', axis=0, tiled=True)]
    ppermute x0 -> x3, waiting for transfers between devices: none -> 52.5 us  [the longest x2 52.5 us: threads_balance(): jax.lax.ppermute(step_out, mesh_dim, perm=tuple(((q, (q + 1) % piece_out)...]
    all_to_all x2, waiting for transfers between devices: 62.6 us -> 56.7 us  [sent_and_summed(): lax.all_to_all(blocks, axis, split_axis=0, concat_axis=0, tiled=True)]
    dynamic_update_slice x0 -> x4, local copies, waits for them, and re-layouts: none -> 4.71 us  [the longest x2 3.08 us: threads_balance(): lax.dynamic_update_slice_in_dim(near, step_out, (odd - h) % piece_out * l...]
    all_to_all x1, starting transfers between devices: 10.7 us -> 14.6 us  [on_device(): lax.all_to_all(expert_out.reshape(n_ep, capacity, width), 'ep', split_axi...]
    ppermute x0 -> x3, starting transfers between devices: none -> 3.59 us  [the longest x2 1.85 us: threads_balance(): jax.lax.ppermute(step_out, mesh_dim, perm=tuple(((q, (q + 1) % piece_out)...]
  transfers between devices with their start and end apart: 5 -> 7, of which waited for: 5 -> 6; matrix products, arithmetic and copies ran while one was open for 2% -> 4% of each run, Pallas kernels for 0% -> 0%
where the time goes in v1:
time: 322 us
  waiting for transfers between devices  162 us (50%)
  blocking collectives  63.2 us (20%)
  starting transfers between devices  28.9 us (9%)
  local copies, waits for them, and re-layouts  27.7 us (9%)
  matrix products  26.1 us (8%)
  other arithmetic  12.4 us (4%)
    all_to_all x1, blocking collectives, on_device(): lax.all_to_all(outgoing, 'ep', split_axis=0, concat_axis=1, tiled=True)  63.2 us
    all_to_all x2, waiting for transfers between devices, sent_and_summed(): lax.all_to_all(blocks, axis, split_axis=0, concat_axis=0, tiled=True)  56.7 us
    ppermute x2, waiting for transfers between devices, threads_balance(): jax.lax.ppermute(step_out, mesh_dim, perm=tuple(((q, (q + 1) % piece_out)...  52.5 us
    all_to_all x1, waiting for transfers between devices, on_device(): lax.all_to_all(expert_out.reshape(n_ep, capacity, width), 'ep', split_axi...  50.1 us
    dot_general x1, matrix products, on_device(): jnp.dot(piece, w_down[0], preferred_element_type=jnp.float32)  17.5 us
    all_to_all x1, starting transfers between devices, on_device(): lax.all_to_all(expert_out.reshape(n_ep, capacity, width), 'ep', split_axi...  14.6 us
    all_to_all x2, starting transfers between devices, sent_and_summed(): lax.all_to_all(blocks, axis, split_axis=0, concat_axis=0, tiled=True)  8.73 us
    dot_general x1, matrix products, on_device(): gate_val = jnp.dot(piece, w_gate[0], preferred_element_type=jnp.float32)  7.17 us
  transfers between devices with their start and end apart: 7, of which 6 were waited for; matrix products, arithmetic and copies ran while one was open for 4% of the time, Pallas kernels for 0%

profile of v1, /device:TPU:8, one launch (start us, length us, event | category | flops | bytes accessed | tf_op | source)
XLA Modules:
  0.0 321.6 jit_solution(17783379644367424700)
XLA Ops:
  7.7 3.0 gather_fusion
  10.7 2.4 reshape.88
  13.1 63.2 %all_to_all.24 = bf16[64,5,2048]{2,1,0:T(8,128)(2,1)} all-to-all(bf16[64,5,2048]{2,1,0:T(8,128)(2,1)S(1)} %reshape.88), channel_id=1, replica_groups=mesh['ep'=64,'tp'=4] {'ep'}, dimensions={0} | all-to-all | bytes 2621440 | tf_op jit(solution)/shard_map/all_to_all | solution.py:85
  76.3 2.6 reshape.89
  80.5 1.7 collective-permute-start.2
  82.2 27.1 %collective-permute-done.1 = bf16[320,2048]{1,0:T(8,128)(2,1)} collective-permute-done((bf16[320,2048]{1,0:T(8,128)(2,1)S(1)}, bf16[320,2048]{1,0:T(8,128)(2,1)}, u32[]{:S(2)}, u32[]{:S(2)}) %collective-permute-start.1) | collective-permute-done | bytes 1310752 | tf_op jit(solution)/shard_map/ppermute | solution.py:102
  113.5 25.4 %collective-permute-done.3 = bf16[320,2048]{1,0:T(8,128)(2,1)} collective-permute-done((bf16[320,2048]{1,0:T(8,128)(2,1)}, bf16[320,2048]{1,0:T(8,128)(2,1)}, u32[]{:S(2)}, u32[]{:S(2)}) %collective-permute-start.3) | collective-permute-done | bytes 1310752 | tf_op jit(solution)/shard_map/ppermute | solution.py:102
  140.4 2.3 copy-done.1
  142.8 7.2 %fusion.5 = f32[1280,896]{1,0:T(8,128)} fusion(bf16[1280,2048]{1,0:T(8,128)(2,1)S(1)} %constant_dynamic-update-slice_fusion, bf16[1,2048,896]{2,1,0:T(8,128)(2,1)S(1)} %copy-done.7), kind=kOutput, calls=%fused_computation.8 | convolution fusion | flops 4697620480 | bytes 13500416 | tf_op jit(solution)/shard_map/dot_general | solution.py:117
  150.0 17.5 %convolution_convert_fusion = bf16[1280,2048]{1,0:T(8,128)(2,1)} fusion(bf16[1,896,2048]{2,1,0:T(8,128)(2,1)} %param.23, f32[1280,896]{1,0:T(8,128)} %fusion.5, bf16[1280,2048]{1,0:T(8,128)(2,1)} %copy-done.1, bf16[1,2048,896]{2,1,0:T(8,128)(2,1)} %param.22), kind=kOutput, calls=%fused_computation.3 | convolution fusion | flops 9404743680 | bytes 22413312 | tf_op jit(solution)/shard_map/dot_general | solution.py:122
  167.5 5.2 %all-to-all-start.2 = ((bf16[4,320,2048]{2,1,0:T(8,128)(2,1)}), bf16[4,320,2048]{2,1,0:T(8,128)(2,1)}, u32[]{:S(2)}, u32[]{:S(2)}) async-start(bf16[4,320,2048]{2,1,0:T(8,128)(2,1)} %bitcast.49), calls=%async_computation.2 | async-start | bytes 10485760 | tf_op jit(solution)/shard_map/all_to_all | solution.py:22
  172.8 1.9 collective-permute-start
  174.8 3.0 collective-permute-done
  179.2 50.7 %all-to-all-done.2 = bf16[4,320,2048]{2,1,0:T(8,128)(2,1)} async-done(((bf16[4,320,2048]{2,1,0:T(8,128)(2,1)}), bf16[4,320,2048]{2,1,0:T(8,128)(2,1)}, u32[]{:S(2)}, u32[]{:S(2)}) %all-to-all-start.2) | async-done | bytes 5242912 | tf_op jit(solution)/shard_map/all_to_all | solution.py:22
  229.9 3.5 %all-to-all-start = ((bf16[4,64,2048]{2,1,0:T(8,128)(2,1)}), bf16[4,64,2048]{2,1,0:T(8,128)(2,1)S(1)}, u32[]{:S(2)}, u32[]{:S(2)}) async-start(bf16[4,64,2048]{2,1,0:T(8,128)(2,1)} %bitcast.3), calls=%async_computation | async-start | bytes 2097152 | tf_op jit(solution)/shard_map/all_to_all | solution.py:22
  233.4 3.6 %reduce_sum.57 = bf16[320,2048]{1,0:T(8,128)(2,1)S(1)} reduce(bf16[4,320,2048]{2,1,0:T(8,128)(2,1)} %all-to-all-done.2, bf16[]{:T(256)} %constant.58.clone.1), dimensions={0}, to_apply=%region_6.7 | reduce | flops 1966080 | bytes 6553602 | tf_op jit(solution)/shard_map/reduce_sum | solution.py:23
  237.0 1.6 reshape.91
  238.7 6.0 %all-to-all-done = bf16[4,64,2048]{2,1,0:T(8,128)(2,1)S(1)} async-done(((bf16[4,64,2048]{2,1,0:T(8,128)(2,1)}), bf16[4,64,2048]{2,1,0:T(8,128)(2,1)S(1)}, u32[]{:S(2)}, u32[]{:S(2)}) %all-to-all-start) | async-done | bytes 1048608 | tf_op jit(solution)/shard_map/all_to_all | solution.py:22
  244.7 14.6 %all-to-all-start.3 = ((bf16[64,5,2048]{2,1,0:T(8,128)(2,1)}), bf16[64,5,2048]{2,1,0:T(8,128)(2,1)}, u32[]{:S(2)}, u32[]{:S(2)}) async-start(bf16[64,5,2048]{2,1,0:T(8,128)(2,1)} %reshape.91), calls=%async_computation.3 | async-start | bytes 4194304 | tf_op jit(solution)/shard_map/all_to_all | solution.py:124
  260.3 50.1 %all-to-all-done.3 = bf16[64,5,2048]{2,1,0:T(8,128)(2,1)} async-done(((bf16[64,5,2048]{2,1,0:T(8,128)(2,1)}), bf16[64,5,2048]{2,1,0:T(8,128)(2,1)}, u32[]{:S(2)}, u32[]{:S(2)}) %all-to-all-start.3) | async-done | bytes 1310752 | tf_op jit(solution)/shard_map/all_to_all | solution.py:124
  310.4 2.6 reshape.92
  313.0 2.3 gather_fusion.1
  315.3 2.4 reshape.93
  317.7 3.9 %multiply_reduce_fusion = bf16[128,2048]{1,0:T(8,128)(2,1)} fusion(f32[128,2,2048]{2,1,0:T(2,128)S(1)} %reshape.93, f32[128,2]{1,0:T(8,128)S(1)} %copy.19), kind=kLoop, calls=%fused_computation.11 | loop fusion | flops 786432 | bytes 2622464 | tf_op jit(solution)/shard_map/reduce_sum | solution.py:128
  (51 shorter events, 16.8 us)
Async XLA Ops:
  0.6 177.1 %copy-start = (bf16[256,2048]{1,0:T(8,128)(2,1)S(1)}, bf16[256,2048]{1,0:T(8,128)(2,1)}, u32[]{:S(2)}) copy-start(bf16[256,2048]{1,0:T(8,128)(2,1)} %param.16) | copy-start | bytes 3145732
  78.9 30.4 %collective-permute-start.1 = (bf16[320,2048]{1,0:T(8,128)(2,1)S(1)}, bf16[320,2048]{1,0:T(8,128)(2,1)}, u32[]{:S(2)}, u32[]{:S(2)}) collective-permute-start(bf16[320,2048]{1,0:T(8,128)(2,1)S(1)} %reshape.89), channel_id=1, source_target_pairs={{0,1},{1,2},{2,3},{3,0},{4,5},{5,6},{6,7},{7,4},{8,9},{9,10},{10,1... | collective-permute-start | bytes 3932168 | tf_op jit(solution)/shard_map/ppermute | solution.py:102
  80.5 31.6 %collective-permute-start.2 = (bf16[320,2048]{1,0:T(8,128)(2,1)S(1)}, bf16[320,2048]{1,0:T(8,128)(2,1)}, u32[]{:S(2)}, u32[]{:S(2)}) collective-permute-start(bf16[320,2048]{1,0:T(8,128)(2,1)S(1)} %reshape.89), channel_id=1, source_target_pairs={{0,3},{1,0},{2,1},{3,2},{4,7},{5,4},{6,5},{7,6},{8,11},{9,8},{10,9... | collective-permute-start | bytes 3932168 | tf_op jit(solution)/shard_map/ppermute | solution.py:110
  109.3 29.7 %collective-permute-start.3 = (bf16[320,2048]{1,0:T(8,128)(2,1)}, bf16[320,2048]{1,0:T(8,128)(2,1)}, u32[]{:S(2)}, u32[]{:S(2)}) collective-permute-start(bf16[320,2048]{1,0:T(8,128)(2,1)} %collective-permute-done.1), channel_id=1, source_target_pairs={{0,1},{1,2},{2,3},{3,0},{4,5},{5,6},{6,7},{7,4},{8,9},{9,10},{10,1... | collective-permute-start | bytes 3932168 | tf_op jit(solution)/shard_map/ppermute | solution.py:102
  110.4 32.4 %copy-start.7 = (bf16[1,2048,896]{2,1,0:T(8,128)(2,1)S(1)}, bf16[1,2048,896]{2,1,0:T(8,128)(2,1)}, u32[]{:S(2)}) copy-start(bf16[1,2048,896]{2,1,0:T(8,128)(2,1)} %param.21) | copy-start | bytes 11010052
  140.4 2.4 copy-start.1
  167.5 5.3 %copy-start.3 = (bf16[256,256]{1,0:T(8,128)(2,1)S(1)}, bf16[256,256]{1,0:T(8,128)(2,1)}, u32[]{:S(2)}) copy-start(bf16[256,256]{1,0:T(8,128)(2,1)} %param.14) | copy-start | bytes 393220
  167.5 5.3 %copy-start.4 = (bf16[256,256]{1,0:T(8,128)(2,1)S(1)}, bf16[256,256]{1,0:T(8,128)(2,1)}, u32[]{:S(2)}) copy-start(bf16[256,256]{1,0:T(8,128)(2,1)} %param.12) | copy-start | bytes 393220
  167.5 7.2 %copy-start.5 = (f32[3,256]{1,0:T(4,128)S(1)}, f32[3,256]{1,0:T(4,128)}, u32[]{:S(2)}) copy-start(f32[3,256]{1,0:T(4,128)} %param.15) | copy-start | bytes 9220
  167.5 10.2 %copy-start.2 = (bf16[256,256]{1,0:T(8,128)(2,1)S(1)}, bf16[256,256]{1,0:T(8,128)(2,1)}, u32[]{:S(2)}) copy-start(bf16[256,256]{1,0:T(8,128)(2,1)} %param.13) | copy-start | bytes 393220
  167.5 62.4 %all-to-all-start.2 = ((bf16[4,320,2048]{2,1,0:T(8,128)(2,1)}), bf16[4,320,2048]{2,1,0:T(8,128)(2,1)}, u32[]{:S(2)}, u32[]{:S(2)}) async-start(bf16[4,320,2048]{2,1,0:T(8,128)(2,1)} %bitcast.49), calls=%async_computation.2 | async-start | bytes 10485760 | tf_op jit(solution)/shard_map/all_to_all | solution.py:22
  172.8 4.9 %collective-permute-start = (f32[2,256]{1,0:T(2,128)S(1)}, f32[2,256]{1,0:T(2,128)S(1)}, u32[]{:S(2)}, u32[]{:S(2)}) collective-permute-start(f32[2,256]{1,0:T(2,128)S(1)} %slice.36), channel_id=1, source_target_pairs={{0,4},{4,8},{8,12},{12,16},{16,20},{20,24},{24,28},{28,32},{32,36}... | collective-permute-start | bytes 6152 | tf_op jit(solution)/shard_map/ppermute | solution.py:12
  229.9 14.8 %all-to-all-start = ((bf16[4,64,2048]{2,1,0:T(8,128)(2,1)}), bf16[4,64,2048]{2,1,0:T(8,128)(2,1)S(1)}, u32[]{:S(2)}, u32[]{:S(2)}) async-start(bf16[4,64,2048]{2,1,0:T(8,128)(2,1)} %bitcast.3), calls=%async_computation | async-start | bytes 2097152 | tf_op jit(solution)/shard_map/all_to_all | solution.py:22
  237.0 22.3 %copy-start.6 = (f32[128,2]{0,1:T(2,128)S(1)}, f32[128,2]{0,1:T(2,128)}, u32[]{:S(2)}) copy-start(f32[128,2]{0,1:T(2,128)} %param.20) | copy-start | bytes 3076
  244.7 65.8 %all-to-all-start.3 = ((bf16[64,5,2048]{2,1,0:T(8,128)(2,1)}), bf16[64,5,2048]{2,1,0:T(8,128)(2,1)}, u32[]{:S(2)}, u32[]{:S(2)}) async-start(bf16[64,5,2048]{2,1,0:T(8,128)(2,1)} %reshape.91), calls=%async_computation.3 | async-start | bytes 4194304 | tf_op jit(solution)/shard_map/all_to_all | solution.py:124
